TPU v7x, 32 devices: a whole 2x2x4 slice. The times are simulated.
32 devices in a mesh: grp: 2 (over y), fs: 4 (over z), tp: 4 (over x, core).
Axes of the slice: x: 2, y: 2, z: 4, core: 2. Of those that a mesh axis runs over, the one named last changes fastest.
Arguments:
- tokens: bfloat16 [2560, 2048], P(('grp', 'fs', 'tp')), parts along dimension 0, may hold values from -6 to 6
- mix_gain: bfloat16 [2048], replicated, may hold values from 0.099609375 to 1.8984375
- val_weight: bfloat16 [2048, 1024], P('fs', 'tp'), may hold values from -4 to 4
- gate_weight: bfloat16 [2048, 1024], P('fs', 'tp'), may hold values from -0.125 to 0.125
- conv_taps: bfloat16 [31, 1024], replicated, may hold values from -1 to 1
- chan_gain: bfloat16 [1024], replicated, may hold values from 0.099609375 to 1.8984375
- out_weight: bfloat16 [1024, 2048], P('tp', 'fs'), may hold values from -0.1875 to 0.1875
- mix_post_gain: bfloat16 [2048], replicated, may hold values from 0.099609375 to 1.8984375
- ffn_gain: bfloat16 [2048], replicated, may hold values from 0.099609375 to 1.8984375
- up_gate_weight: bfloat16 [2048, 5120], P('fs', 'tp'), may hold values from -0.125 to 0.125
- up_val_weight: bfloat16 [2048, 5120], P('fs', 'tp'), may hold values from -0.125 to 0.125
- ffn_taps: bfloat16 [2, 3, 5120], replicated, may hold values from -3.5 to 3.5
- down_weight: bfloat16 [5120, 2048], P('tp', 'fs'), may hold values from -0.078125 to 0.078125
- ffn_post_gain: bfloat16 [2048], replicated, may hold values from 0.099609375 to 1.8984375
Outputs:
- layer_out: bfloat16 [2560, 2048], P(('grp', 'fs', 'tp')), parts along dimension 0
There are 2 independent parts, one for each index of `grp`. A program takes and returns all parts, laid end to end along the dimension named above; an argument that names none is the same for every part. Nothing has to cross between parts.
All inputs are finite; a program needn't handle non-finite values.
Results may differ from a plain program's by a relative error of at most 0.019.
Values may be sent and summed in bfloat16 or wider, within the bound.
A program may use at most 64 MiB of HBM per device.

v0:
```python
import jax
import jax.numpy as jnp
from jax import lax
from jax.sharding import PartitionSpec as P

LEN = 64
norm_epsilon = 1e-06
chan_epsilon = 1e-05


def rms_scale(values, gain):
    inverse = lax.rsqrt(jnp.mean(values * values, axis=-1, keepdims=True) + norm_epsilon)
    return values * inverse * gain.astype(jnp.float32)


def depthwise(signal, tap_table):
    taps_count = tap_table.shape[0]
    channels = signal.shape[1]
    shaped = signal.astype(jnp.float32).reshape(signal.shape[0] // LEN, LEN, channels)
    padded = jnp.pad(shaped, ((0, 0), (taps_count - 1, 0), (0, 0)))
    tap_values = tap_table.astype(jnp.float32)
    result = jnp.zeros(shaped.shape, jnp.float32)
    for offset in range(taps_count):
        result = result + padded[:, offset : offset + LEN, :] * tap_values[offset]
    return result.reshape(signal.shape[0], channels)


def make_adder(left, pieces):
    first = jnp.dot(left, pieces[0], preferred_element_type=jnp.float32)
    second = jnp.dot(left, pieces[1], preferred_element_type=jnp.float32)
    return (first, second)


def make_rows_product(left, weight):
    return jnp.dot(left, weight, preferred_element_type=jnp.float32)


def shards(
    tokens,
    mix_gain,
    val_weight,
    gate_weight,
    conv_taps,
    chan_gain,
    out_weight,
    mix_post_gain,
    ffn_gain,
    up_gate_weight,
    up_val_weight,
    ffn_taps,
    down_weight,
    ffn_post_gain,
):
    member = lax.axis_index("tp")
    normed_own = rms_scale(tokens.astype(jnp.float32), mix_gain).astype(jnp.bfloat16)
    normed = lax.all_gather(normed_own, "tp", axis=0, tiled=True)
    local_ch = val_weight.shape[1]
    values, gate_sums = make_adder(
        normed,
        (
            lax.all_gather(val_weight, "fs", axis=0, tiled=True),
            lax.all_gather(gate_weight, "fs", axis=0, tiled=True),
        ),
    )
    glu_out = (values * jax.nn.sigmoid(gate_sums)).astype(jnp.bfloat16)
    own_taps = lax.dynamic_slice_in_dim(conv_taps, member * local_ch, local_ch, 1)
    conv_out = depthwise(glu_out, own_taps)
    totals, squares = lax.psum(
        (jnp.sum(conv_out, axis=1), jnp.sum(conv_out * conv_out, axis=1)), "tp"
    )
    all_channels = chan_gain.shape[0]
    chan_mean = totals[:, None] / all_channels
    chan_var = squares[:, None] / all_channels - chan_mean * chan_mean
    own_gain = lax.dynamic_slice_in_dim(chan_gain, member * local_ch, local_ch, 0).astype(
        jnp.float32
    )
    activated = jax.nn.silu((conv_out - chan_mean) * lax.rsqrt(chan_var + chan_epsilon) * own_gain)
    activated = activated.astype(jnp.bfloat16)
    out_full = lax.all_gather(out_weight, "fs", axis=1, tiled=True)
    mixed_sum = lax.psum_scatter(
        make_rows_product(activated, out_full).astype(jnp.bfloat16),
        "tp",
        scatter_dimension=0,
        tiled=True,
    ).astype(jnp.float32)
    residual = (tokens.astype(jnp.float32) + rms_scale(mixed_sum, mix_post_gain)).astype(
        jnp.bfloat16
    )
    normed_share = rms_scale(residual.astype(jnp.float32), ffn_gain).astype(jnp.bfloat16)
    normed_ffn = lax.all_gather(normed_share, "tp", axis=0, tiled=True)
    local_ff = up_gate_weight.shape[1]
    own_ffn_taps = lax.dynamic_slice_in_dim(ffn_taps, member * local_ff, local_ff, 2)
    gate_full, val_full = (
        lax.all_gather(up_gate_weight, "fs", axis=0, tiled=True),
        lax.all_gather(up_val_weight, "fs", axis=0, tiled=True),
    )
    up_gate = jnp.dot(normed_ffn, gate_full, preferred_element_type=jnp.float32).astype(
        jnp.bfloat16
    )
    up_val = jnp.dot(normed_ffn, val_full, preferred_element_type=jnp.float32).astype(jnp.bfloat16)
    gate_conv = depthwise(up_gate, own_ffn_taps[0])
    val_conv = depthwise(up_val, own_ffn_taps[1])
    hidden = (jax.nn.gelu(gate_conv, approximate=True) * val_conv).astype(jnp.bfloat16)
    down_full = lax.all_gather(down_weight, "fs", axis=1, tiled=True)
    ffn_sum = lax.psum_scatter(
        make_rows_product(hidden, down_full).astype(jnp.bfloat16),
        "tp",
        scatter_dimension=0,
        tiled=True,
    ).astype(jnp.float32)
    return (residual.astype(jnp.float32) + rms_scale(ffn_sum, ffn_post_gain)).astype(jnp.bfloat16)


def solution(mesh):
    return jax.shard_map(
        shards,
        mesh=mesh,
        in_specs=(
            P(("grp", "fs", "tp"), None),
            P(),
            P("fs", "tp"),
            P("fs", "tp"),
            P(),
            P(),
            P("tp", "fs"),
            P(),
            P(),
            P("fs", "tp"),
            P("fs", "tp"),
            P(),
            P("tp", "fs"),
            P(),
        ),
        out_specs=P(("grp", "fs", "tp"), None),
        check_vma=False,
    )
```

profile of v0, /device:TPU:0, one launch (start us, length us, event | category | flops | bytes accessed | tf_op | source)
XLA Modules:
  0.0 503.6 jit_solution(17224619364062690328)
XLA Ops:
  6.5 0.0 all-gather.11.cloned.1.call-start
  6.5 0.7 all-gather.11.cloned.1.call-update
  7.3 0.0 all-gather.9.cloned.1.call-start
  7.3 0.7 convert_element_type.82
  8.0 1.1 fusion.26
  9.1 1.8 fusion.28
  11.0 0.0 all-gather.9.cloned.1.call-update
  11.0 0.0 all-gather.13.cloned.1.call-start
  11.1 0.7 all-gather.13.cloned.1.call-update
  11.8 0.0 all-gather.15.cloned.1.call-start
  11.8 0.5 all-gather.15.cloned.1.call-update
  12.3 0.0 reduce-scatter.3.cloned.1.call-start
  12.4 0.7 dynamic-slice_convert_fusion
  13.1 0.8 dynamic-slice_convert_fusion.3
  13.9 25.7 %all-gather.11.cloned.1.call-done = bf16[2048,256]{1,0:T(8,128)(2,1)} async-done(((bf16[512,256]{1,0:T(8,128)(2,1)}), bf16[2048,256]{1,0:T(8,128)(2,1)}) %all-gather.11.cloned.1.call-update) | async-done | bytes 1048592 | tf_op jit(solution)/shard_map/all_gather | solution.py:61
  39.7 19.1 %all-gather.9.cloned.1.call-done = bf16[320,2048]{1,0:T(8,128)(2,1)} async-done(((bf16[80,2048]{1,0:T(8,128)(2,1)}), bf16[320,2048]{1,0:T(8,128)(2,1)}) %all-gather.9.cloned.1.call-update) | async-done | bytes 1310736 | tf_op jit(solution)/shard_map/all_gather | solution.py:56
  58.8 2.2 fusion.101
  61.0 27.4 %all-gather.13.cloned.1.call-done = bf16[2048,256]{1,0:T(8,128)(2,1)} async-done(((bf16[512,256]{1,0:T(8,128)(2,1)}), bf16[2048,256]{1,0:T(8,128)(2,1)}) %all-gather.13.cloned.1.call-update) | async-done | bytes 1048592 | tf_op jit(solution)/shard_map/all_gather | solution.py:62
  88.4 1.7 fusion.21
  90.2 1.2 fusion.96
  91.4 0.1 reduce_sum.60
  91.5 0.1 reduce_sum.62
  91.5 6.1 %all-reduce.3 = (f32[320]{0:T(512)S(1)}, f32[320]{0:T(512)S(1)}) all-reduce(f32[320]{0:T(512)S(1)} %reduce_sum.62, f32[320]{0:T(512)S(1)} %reduce_sum.60), channel_id=1, replica_groups=mesh['grp'=2,'fs'=4,'tp'=4] {'tp'}, use_global_device_ids=true, to_apply=%region_4.5 | all-reduce | flops 640 | bytes 5120 | tf_op jit(solution)/shard_map/psum | solution.py:68
  97.6 0.2 multiply_convert_fusion
  97.8 0.0 copy-start.2
  97.8 0.0 copy-start.3
  97.8 0.0 copy-start
  97.8 19.4 %all-gather.15.cloned.1.call-done = bf16[256,2048]{1,0:T(8,128)(2,1)} async-done(((bf16[256,512]{1,0:T(8,128)(2,1)}), bf16[256,2048]{1,0:T(8,128)(2,1)}) %all-gather.15.cloned.1.call-update) | async-done | bytes 1048592 | tf_op jit(solution)/shard_map/all_gather | solution.py:79
  117.2 2.8 convolution_convert_fusion.3
  120.0 0.0 reduce-scatter.3.cloned.1.call-update
  120.0 0.0 all-gather.17.cloned.1.call-start
  120.1 0.0 copy-done.3
  120.1 25.9 %reduce-scatter.3.cloned.1.call-done = bf16[80,2048]{1,0:T(8,128)(2,1)} async-done(((bf16[320,2048]{1,0:T(8,128)(2,1)}), bf16[80,2048]{1,0:T(8,128)(2,1)}) %reduce-scatter.3.cloned.1.call-update) | async-done | bytes 327696 | tf_op jit(solution)/shard_map/reduce_scatter | solution.py:80
  146.0 1.1 fusion.22
  147.1 0.0 copy-done
  147.1 1.3 fusion.30
  148.5 0.9 fusion.32
  149.3 0.0 all-gather.17.cloned.1.call-update
  149.4 0.0 all-gather.19.cloned.1.call-start
  149.4 0.7 all-gather.19.cloned.1.call-update
  150.1 0.0 copy-start.1
  150.1 0.0 all-gather.21.cloned.1.call-start
  150.2 0.7 all-gather.21.cloned.1.call-update
  150.9 0.0 all-gather.23.cloned.1.call-start
  150.9 0.7 all-gather.23.cloned.1.call-update
  151.6 0.0 reduce-scatter.5.cloned.1.call-start
  151.7 0.1 dynamic-slice_convert_fusion.2
  151.9 15.8 %all-gather.17.cloned.1.call-done = bf16[320,2048]{1,0:T(8,128)(2,1)} async-done(((bf16[80,2048]{1,0:T(8,128)(2,1)}), bf16[320,2048]{1,0:T(8,128)(2,1)}) %all-gather.17.cloned.1.call-update) | async-done | bytes 1310736 | tf_op jit(solution)/shard_map/all_gather | solution.py:90
  167.7 99.6 %all-gather.19.cloned.1.call-done = bf16[2048,1280]{1,0:T(8,128)(2,1)} async-done(((bf16[512,1280]{1,0:T(8,128)(2,1)}), bf16[2048,1280]{1,0:T(8,128)(2,1)}) %all-gather.19.cloned.1.call-update) | async-done | bytes 5242896 | tf_op jit(solution)/shard_map/all_gather | solution.py:94
  267.3 4.8 convolution_convert_fusion.2
  272.1 0.1 convert.4
  272.2 93.1 %all-gather.21.cloned.1.call-done = bf16[2048,1280]{1,0:T(8,128)(2,1)} async-done(((bf16[512,1280]{1,0:T(8,128)(2,1)}), bf16[2048,1280]{1,0:T(8,128)(2,1)}) %all-gather.21.cloned.1.call-update) | async-done | bytes 5242896 | tf_op jit(solution)/shard_map/all_gather | solution.py:95
  365.3 0.0 copy-done.6
  365.3 4.3 convolution_convert_fusion.1
  369.7 0.1 convert.5
  369.8 1.0 fusion.2
  370.8 0.6 fusion.16
  371.3 0.0 copy-start.4
  371.3 92.0 %all-gather.23.cloned.1.call-done = bf16[1280,2048]{1,0:T(8,128)(2,1)} async-done(((bf16[1280,512]{1,0:T(8,128)(2,1)}), bf16[1280,2048]{1,0:T(8,128)(2,1)}) %all-gather.23.cloned.1.call-update) | async-done | bytes 5242896 | tf_op jit(solution)/shard_map/all_gather | solution.py:104
  463.3 5.5 %convolution_convert_fusion = bf16[320,2048]{1,0:T(8,128)(2,1)} fusion(bf16[320,1280]{1,0:T(8,128)(2,1)S(1)} %fusion.16, bf16[1280,2048]{1,0:T(8,128)(2,1)} %all-gather.23.cloned.1.call-done), kind=kOutput, calls=%fused_computation | convolution fusion | flops 1678376960 | bytes 7372800 | tf_op jit(solution)/shard_map/dot_general | solution.py:35
  468.8 0.0 reduce-scatter.5.cloned.1.call-update
  468.8 24.9 %reduce-scatter.5.cloned.1.call-done = bf16[80,2048]{1,0:T(8,128)(2,1)} async-done(((bf16[320,2048]{1,0:T(8,128)(2,1)}), bf16[80,2048]{1,0:T(8,128)(2,1)}) %reduce-scatter.5.cloned.1.call-update) | async-done | bytes 327696 | tf_op jit(solution)/shard_map/reduce_scatter | solution.py:105
  493.7 1.1 fusion.24
  494.9 1.9 fusion.33
  (19 shorter events, 0.2 us)
Async XLA Ops:
  6.5 33.1 %all-gather.11.cloned.1.call-start = ((), (), s32[]{:S(2)}) async-start(), calls=%async_computation.3 | async-start | bytes 1310720 | tf_op jit(solution)/shard_map/all_gather | solution.py:61
  7.3 51.5 %all-gather.9.cloned.1.call-start = ((), (), s32[]{:S(2)}) async-start(), calls=%async_computation.2 | async-start | bytes 1638400 | tf_op jit(solution)/shard_map/all_gather | solution.py:56
  11.0 77.4 %all-gather.13.cloned.1.call-start = ((), (), s32[]{:S(2)}) async-start(), calls=%async_computation.4 | async-start | bytes 1310720 | tf_op jit(solution)/shard_map/all_gather | solution.py:62
  11.8 105.4 %all-gather.15.cloned.1.call-start = ((), (), s32[]{:S(2)}) async-start(), calls=%async_computation.5 | async-start | bytes 1310720 | tf_op jit(solution)/shard_map/all_gather | solution.py:79
  12.3 133.6 %reduce-scatter.3.cloned.1.call-start = ((), (), s32[]{:S(2)}) async-start(), calls=%async_computation.6 | async-start | bytes 1638400 | tf_op jit(solution)/shard_map/reduce_scatter | solution.py:80
  58.8 29.6 %copy-start.5 = (bf16[320,2048]{1,0:T(8,128)(2,1)S(1)}, bf16[320,2048]{1,0:T(8,128)(2,1)}, u32[]{:S(2)}) copy-start(bf16[320,2048]{1,0:T(8,128)(2,1)} %all-gather.9.cloned.1.call-done) | copy-start | bytes 3932164
  97.8 22.3 %copy-start.2 = (bf16[2048]{0:T(1024)(128)(2,1)S(1)}, bf16[2048]{0:T(1024)(128)(2,1)}, u32[]{:S(2)}) copy-start(bf16[2048]{0:T(1024)(128)(2,1)} %param.21) | copy-start | bytes 12292
  97.8 22.3 %copy-start.3 = (bf16[2048]{0:T(1024)(128)(2,1)S(1)}, bf16[2048]{0:T(1024)(128)(2,1)}, u32[]{:S(2)}) copy-start(bf16[2048]{0:T(1024)(128)(2,1)} %param.22) | copy-start | bytes 12292
  97.8 49.3 %copy-start = (bf16[80,2048]{1,0:T(8,128)(2,1)S(1)}, bf16[80,2048]{1,0:T(8,128)(2,1)}, u32[]{:S(2)}) copy-start(bf16[80,2048]{1,0:T(8,128)(2,1)} %param.14) | copy-start | bytes 983044
  120.0 47.7 %all-gather.17.cloned.1.call-start = ((), (), s32[]{:S(2)}) async-start(), calls=%async_computation.7 | async-start | bytes 1638400 | tf_op jit(solution)/shard_map/all_gather | solution.py:90
  149.4 118.0 %all-gather.19.cloned.1.call-start = ((), (), s32[]{:S(2)}) async-start(), calls=%async_computation.8 | async-start | bytes 6553600 | tf_op jit(solution)/shard_map/all_gather | solution.py:94
  150.1 1.5 copy-start.1
  150.1 215.2 %all-gather.21.cloned.1.call-start = ((), (), s32[]{:S(2)}) async-start(), calls=%async_computation.9 | async-start | bytes 6553600 | tf_op jit(solution)/shard_map/all_gather | solution.py:95
  150.9 312.4 %all-gather.23.cloned.1.call-start = ((), (), s32[]{:S(2)}) async-start(), calls=%async_computation.10 | async-start | bytes 6553600 | tf_op jit(solution)/shard_map/all_gather | solution.py:104
  151.6 342.1 %reduce-scatter.5.cloned.1.call-start = ((), (), s32[]{:S(2)}) async-start(), calls=%async_computation.11 | async-start | bytes 1638400 | tf_op jit(solution)/shard_map/reduce_scatter | solution.py:105
  272.1 93.2 %copy-start.6 = (bf16[320,2048]{1,0:T(8,128)(2,1)S(1)}, bf16[320,2048]{1,0:T(8,128)(2,1)}, u32[]{:S(2)}) copy-start(bf16[320,2048]{1,0:T(8,128)(2,1)} %all-gather.17.cloned.1.call-done) | copy-start | bytes 3932164
  371.3 97.5 %copy-start.4 = (bf16[2048]{0:T(1024)(128)(2,1)S(1)}, bf16[2048]{0:T(1024)(128)(2,1)}, u32[]{:S(2)}) copy-start(bf16[2048]{0:T(1024)(128)(2,1)} %param.27) | copy-start | bytes 12292
Sparse Core Ops, SparseCore 0:
  8.9 30.7 all-gather.10
  41.2 17.5 all-gather.8
  60.4 27.9 all-gather.12
  89.8 27.3 all-gather.14
  120.1 25.7 reduce-scatter.2
  149.5 18.1 all-gather.16
  169.3 98.0 all-gather.18
  268.9 96.3 all-gather.20
  366.9 96.3 all-gather.22
  468.9 24.7 reduce-scatter.4
where the time goes:
time: 504 us
  waiting for transfers between devices  447 us (89%)
  matrix products  21.4 us (4%)
  other arithmetic  14.9 us (3%)
  between operations  13.8 us (3%)
  blocking collectives  6.05 us (1%)
    all_gather x1, waiting for transfers between devices, shards(): lax.all_gather(up_gate_weight, 'fs', axis=0, tiled=True)  99.6 us
    all_gather x1, waiting for transfers between devices, shards(): lax.all_gather(up_val_weight, 'fs', axis=0, tiled=True)  93.1 us
    all_gather x1, waiting for transfers between devices, shards(): down_full = lax.all_gather(down_weight, 'fs', axis=1, tiled=True)  92 us
    all_gather x1, waiting for transfers between devices, shards(): lax.all_gather(gate_weight, 'fs', axis=0, tiled=True)  27.4 us
    reduce_scatter x1, waiting for transfers between devices, shards(): lax.psum_scatter(make_rows_product(activated, out_full).astype(jnp.bfloat...  25.9 us
    all_gather x1, waiting for transfers between devices, shards(): lax.all_gather(val_weight, 'fs', axis=0, tiled=True)  25.7 us
    reduce_scatter x1, waiting for transfers between devices, shards(): lax.psum_scatter(make_rows_product(hidden, down_full).astype(jnp.bfloat16...  24.9 us
    all_gather x1, waiting for transfers between devices, shards(): out_full = lax.all_gather(out_weight, 'fs', axis=1, tiled=True)  19.4 us
  transfers between devices with their start and end apart: 10, of which 10 were waited for; matrix products, arithmetic and copies ran while one was open for 4% of the time, Pallas kernels for 0%

commit v1 on v0

--- a/solution.py
+++ b/solution.py
@@ -101,7 +101,12 @@
     gate_conv = depthwise(up_gate, own_ffn_taps[0])
     val_conv = depthwise(up_val, own_ffn_taps[1])
     hidden = (jax.nn.gelu(gate_conv, approximate=True) * val_conv).astype(jnp.bfloat16)
-    down_full = lax.all_gather(down_weight, "fs", axis=1, tiled=True)
+    ring = [down_weight]
+    for hop in range(3):
+        ring.append(lax.ppermute(ring[-1], "fs", [(dev, (dev + 1) % 4) for dev in range(4)]))
+    down_full = jnp.roll(
+        jnp.concatenate(ring[::-1], axis=1), (lax.axis_index("fs") + 1) * ring[0].shape[1], axis=1
+    )
     ffn_sum = lax.psum_scatter(
         make_rows_product(hidden, down_full).astype(jnp.bfloat16),
         "tp",

time: 504 us -> 463 us (0.919)
  waiting for transfers between devices: 447 us -> 355 us
  starting transfers between devices: 0.36 us -> 35.5 us
  local copies, waits for them, and re-layouts: 0.3 us -> 15.8 us
    ppermute x0 -> x3, waiting for transfers between devices: none -> 138 us  [shards(): lax.ppermute(ring[-1], 'fs', [(dev, (dev + 1) % 4) for dev in range(4)])]
    all_gather x1, waiting for transfers between devices: 99.6 us -> 0.01 us  [shards(): lax.all_gather(up_gate_weight, 'fs', axis=0, tiled=True)]
    all_gather x1 -> x0, waiting for transfers between devices: 92 us -> none  [shards(): down_full = lax.all_gather(down_weight, 'fs', axis=1, tiled=True)]
    ppermute x0 -> x3, starting transfers between devices: none -> 35.2 us  [shards(): lax.ppermute(ring[-1], 'fs', [(dev, (dev + 1) % 4) for dev in range(4)])]
    all_gather x1, waiting for transfers between devices: 93.1 us -> 71.8 us  [shards(): lax.all_gather(up_val_weight, 'fs', axis=0, tiled=True)]
    all_gather x1, waiting for transfers between devices: 15.8 us -> 0.01 us  [shards(): normed_ffn = lax.all_gather(normed_share, 'tp', axis=0, tiled=True)]
    unnamed x14 -> x21, local copies, waits for them, and re-layouts: 0.04 us -> 14.3 us
  transfers between devices with their start and end apart: 10 -> 12, of which waited for: 10 -> 10; matrix products, arithmetic and copies ran while one was open for 4% -> 7% of each run, Pallas kernels for 0% -> 0%
where the time goes in v1:
time: 463 us
  waiting for transfers between devices  355 us (77%)
  starting transfers between devices  35.5 us (8%)
  matrix products  21.8 us (5%)
  local copies, waits for them, and re-layouts  15.8 us (3%)
  other arithmetic  14.9 us (3%)
  between operations  13.5 us (3%)
  blocking collectives  6.05 us (1%)
    ppermute x3, waiting for transfers between devices, shards(): lax.ppermute(ring[-1], 'fs', [(dev, (dev + 1) % 4) for dev in range(4)])  138 us
    all_gather x1, waiting for transfers between devices, shards(): lax.all_gather(up_val_weight, 'fs', axis=0, tiled=True)  71.8 us
    ppermute x3, starting transfers between devices, shards(): lax.ppermute(ring[-1], 'fs', [(dev, (dev + 1) % 4) for dev in range(4)])  35.2 us
    all_gather x1, waiting for transfers between devices, shards(): lax.all_gather(gate_weight, 'fs', axis=0, tiled=True)  27.4 us
    reduce_scatter x1, waiting for transfers between devices, shards(): lax.psum_scatter(make_rows_product(activated, out_full).astype(jnp.bfloat...  25.9 us
    all_gather x1, waiting for transfers between devices, shards(): lax.all_gather(val_weight, 'fs', axis=0, tiled=True)  25.7 us
    reduce_scatter x1, waiting for transfers between devices, shards(): lax.psum_scatter(make_rows_product(hidden, down_full).astype(jnp.bfloat16...  24.9 us
    all_gather x1, waiting for transfers between devices, shards(): out_full = lax.all_gather(out_weight, 'fs', axis=1, tiled=True)  19.4 us
  transfers between devices with their start and end apart: 12, of which 10 were waited for; matrix products, arithmetic and copies ran while one was open for 7% of the time, Pallas kernels for 0%

profile of v1, /device:TPU:0, one launch (start us, length us, event | category | flops | bytes accessed | tf_op | source)
XLA Modules:
  0.0 462.6 jit_solution(6617423647172538523)
XLA Ops:
  6.5 0.7 all-gather.10.cloned.1.call-update
  7.3 0.0 all-gather.8.cloned.1.call-start
  7.3 0.7 convert_element_type.82
  8.0 1.1 fusion.31
  9.1 1.8 fusion.33
  11.0 0.0 all-gather.8.cloned.1.call-update
  11.0 0.0 all-gather.12.cloned.1.call-start
  11.1 0.7 all-gather.12.cloned.1.call-update
  11.8 0.0 all-gather.14.cloned.1.call-start
  11.8 0.5 all-gather.14.cloned.1.call-update
  12.3 0.0 reduce-scatter.3.cloned.1.call-start
  12.4 0.7 dynamic-slice_convert_fusion
  13.1 0.8 dynamic-slice_convert_fusion.3
  13.9 25.7 %all-gather.10.cloned.1.call-done = bf16[2048,256]{1,0:T(8,128)(2,1)} async-done(((bf16[512,256]{1,0:T(8,128)(2,1)}), bf16[2048,256]{1,0:T(8,128)(2,1)}) %all-gather.10.cloned.1.call-update) | async-done | bytes 1048592 | tf_op jit(solution)/shard_map/all_gather | solution.py:61
  39.7 19.1 %all-gather.8.cloned.1.call-done = bf16[320,2048]{1,0:T(8,128)(2,1)} async-done(((bf16[80,2048]{1,0:T(8,128)(2,1)}), bf16[320,2048]{1,0:T(8,128)(2,1)}) %all-gather.8.cloned.1.call-update) | async-done | bytes 1310736 | tf_op jit(solution)/shard_map/all_gather | solution.py:56
  58.8 2.2 fusion.107
  61.0 27.4 %all-gather.12.cloned.1.call-done = bf16[2048,256]{1,0:T(8,128)(2,1)} async-done(((bf16[512,256]{1,0:T(8,128)(2,1)}), bf16[2048,256]{1,0:T(8,128)(2,1)}) %all-gather.12.cloned.1.call-update) | async-done | bytes 1048592 | tf_op jit(solution)/shard_map/all_gather | solution.py:62
  88.4 1.7 fusion.26
  90.2 1.2 fusion.102
  91.4 0.1 reduce_sum.60
  91.5 0.1 reduce_sum.62
  91.5 6.0 %all-reduce.3 = (f32[320]{0:T(512)S(1)}, f32[320]{0:T(512)S(1)}) all-reduce(f32[320]{0:T(512)S(1)} %reduce_sum.62, f32[320]{0:T(512)S(1)} %reduce_sum.60), channel_id=1, replica_groups=mesh['grp'=2,'fs'=4,'tp'=4] {'tp'}, use_global_device_ids=true, to_apply=%region_4.5 | all-reduce | flops 640 | bytes 5120 | tf_op jit(solution)/shard_map/psum | solution.py:68
  97.6 0.2 multiply_convert_fusion
  97.8 19.4 %all-gather.14.cloned.1.call-done = bf16[256,2048]{1,0:T(8,128)(2,1)} async-done(((bf16[256,512]{1,0:T(8,128)(2,1)}), bf16[256,2048]{1,0:T(8,128)(2,1)}) %all-gather.14.cloned.1.call-update) | async-done | bytes 1048592 | tf_op jit(solution)/shard_map/all_gather | solution.py:79
  117.2 2.8 convolution_convert_fusion.2
  120.0 0.0 reduce-scatter.3.cloned.1.call-update
  120.0 0.0 all-gather.16.cloned.1.call-start
  120.1 25.9 %reduce-scatter.3.cloned.1.call-done = bf16[80,2048]{1,0:T(8,128)(2,1)} async-done(((bf16[320,2048]{1,0:T(8,128)(2,1)}), bf16[80,2048]{1,0:T(8,128)(2,1)}) %reduce-scatter.3.cloned.1.call-update) | async-done | bytes 327696 | tf_op jit(solution)/shard_map/reduce_scatter | solution.py:80
  146.0 1.1 fusion.27
  147.1 1.3 fusion.35
  148.5 0.9 fusion.37
  149.3 0.0 all-gather.16.cloned.1.call-update
  149.4 0.0 all-gather.18.cloned.1.call-start
  149.4 0.7 all-gather.18.cloned.1.call-update
  150.1 0.0 all-gather.20.cloned.1.call-start
  150.2 0.7 all-gather.20.cloned.1.call-update
  150.9 0.0 reduce-scatter.5.cloned.1.call-start
  150.9 1.5 collective-permute-start
  152.5 32.1 %collective-permute-done = bf16[1280,512]{1,0:T(8,128)(2,1)S(1)} collective-permute-done((bf16[1280,512]{1,0:T(8,128)(2,1)S(1)}, bf16[1280,512]{1,0:T(8,128)(2,1)S(1)}, u32[]{:S(2)}, u32[]{:S(2)}) %collective-permute-start) | collective-permute-done | bytes 1310752 | tf_op jit(solution)/shard_map/ppermute | solution.py:106
  184.6 4.5 collective-permute-start.1
  189.1 57.1 %collective-permute-done.1 = bf16[1280,512]{1,0:T(8,128)(2,1)} collective-permute-done((bf16[1280,512]{1,0:T(8,128)(2,1)S(1)}, bf16[1280,512]{1,0:T(8,128)(2,1)}, u32[]{:S(2)}, u32[]{:S(2)}) %collective-permute-start.1) | collective-permute-done | bytes 1310752 | tf_op jit(solution)/shard_map/ppermute | solution.py:106
  246.1 29.1 %collective-permute-start.2 = (bf16[1280,512]{1,0:T(8,128)(2,1)}, bf16[1280,512]{1,0:T(8,128)(2,1)}, u32[]{:S(2)}, u32[]{:S(2)}) collective-permute-start(bf16[1280,512]{1,0:T(8,128)(2,1)} %collective-permute-done.1), channel_id=1, source_target_pairs={{0,4},{4,8},{8,12},{12,0},{1,5},{5,9},{9,13},{13,1},{2,6},{6,10},{... | collective-permute-start | bytes 3932168 | tf_op jit(solution)/shard_map/ppermute | solution.py:106
  275.3 0.1 dynamic-slice_convert_fusion.2
  275.5 48.4 %collective-permute-done.2 = bf16[1280,512]{1,0:T(8,128)(2,1)} collective-permute-done((bf16[1280,512]{1,0:T(8,128)(2,1)}, bf16[1280,512]{1,0:T(8,128)(2,1)}, u32[]{:S(2)}, u32[]{:S(2)}) %collective-permute-start.2) | collective-permute-done | bytes 1310752 | tf_op jit(solution)/shard_map/ppermute | solution.py:106
  323.9 2.7 constant_dynamic-update-slice_fusion.7
  326.6 2.7 constant_dynamic-update-slice_fusion.6
  329.3 1.2 constant_dynamic-update-slice_fusion.5
  330.5 1.2 constant_dynamic-update-slice_fusion.4
  331.8 2.5 constant_dynamic-update-slice_fusion.3
  334.3 2.6 constant_dynamic-update-slice_fusion.2
  336.9 1.3 constant_dynamic-update-slice_fusion.1
  338.2 1.2 constant_dynamic-update-slice_fusion
  339.4 4.8 %convolution_convert_fusion.1 = bf16[320,1280]{1,0:T(8,128)(2,1)S(1)} fusion(bf16[320,2048]{1,0:T(8,128)(2,1)} %all-gather.16.cloned.1.call-done, bf16[2048,1280]{1,0:T(8,128)(2,1)} %all-gather.18.cloned.1.call-done), kind=kOutput, calls=%fused_computation.4 | convolution fusion | flops 1678131200 | bytes 7372800 | tf_op jit(solution)/shard_map/dot_general | solution.py:97
  344.3 0.1 convert.4
  344.4 71.8 %all-gather.20.cloned.1.call-done = bf16[2048,1280]{1,0:T(8,128)(2,1)} async-done(((bf16[512,1280]{1,0:T(8,128)(2,1)}), bf16[2048,1280]{1,0:T(8,128)(2,1)}) %all-gather.20.cloned.1.call-update) | async-done | bytes 5242896 | tf_op jit(solution)/shard_map/all_gather | solution.py:95
  416.2 4.7 %convolution_convert_fusion = bf16[320,1280]{1,0:T(8,128)(2,1)S(1)} fusion(bf16[320,2048]{1,0:T(8,128)(2,1)} %all-gather.16.cloned.1.call-done, bf16[2048,1280]{1,0:T(8,128)(2,1)} %all-gather.20.cloned.1.call-done), kind=kOutput, calls=%fused_computation.3 | convolution fusion | flops 1678131200 | bytes 7372800 | tf_op jit(solution)/shard_map/dot_general | solution.py:100
  421.0 0.1 convert.5
  421.1 1.0 fusion.7
  422.1 0.6 fusion.21
  422.6 5.5 %fusion.2 = bf16[320,2048]{1,0:T(8,128)(2,1)} fusion(bf16[320,1280]{1,0:T(8,128)(2,1)S(1)} %fusion.21, bf16[1280,4096]{1,0:T(8,128)(2,1)} %constant_dynamic-update-slice_fusion, s32[]{:T(128)S(6)} %select_n.23), kind=kOutput, calls=%fused_computation.2 | convolution fusion | flops 1678376960 | bytes 7372804 | tf_op jit(solution)/shard_map/dot_general | solution.py:35
  428.1 0.0 reduce-scatter.5.cloned.1.call-update
  428.1 24.9 %reduce-scatter.5.cloned.1.call-done = bf16[80,2048]{1,0:T(8,128)(2,1)} async-done(((bf16[320,2048]{1,0:T(8,128)(2,1)}), bf16[80,2048]{1,0:T(8,128)(2,1)}) %reduce-scatter.5.cloned.1.call-update) | async-done | bytes 327696 | tf_op jit(solution)/shard_map/reduce_scatter | solution.py:110
  453.1 1.1 fusion.29
  454.2 1.9 fusion.38
  (30 shorter events, 0.2 us)
Async XLA Ops:
  6.5 33.1 %all-gather.10.cloned.1.call-start = ((), (), s32[]{:S(2)}) async-start(), calls=%async_computation.3 | async-start | bytes 1310720 | tf_op jit(solution)/shard_map/all_gather | solution.py:61
  7.3 51.5 %all-gather.8.cloned.1.call-start = ((), (), s32[]{:S(2)}) async-start(), calls=%async_computation.2 | async-start | bytes 1638400 | tf_op jit(solution)/shard_map/all_gather | solution.py:56
  11.0 77.4 %all-gather.12.cloned.1.call-start = ((), (), s32[]{:S(2)}) async-start(), calls=%async_computation.4 | async-start | bytes 1310720 | tf_op jit(solution)/shard_map/all_gather | solution.py:62
  11.8 105.4 %all-gather.14.cloned.1.call-start = ((), (), s32[]{:S(2)}) async-start(), calls=%async_computation.5 | async-start | bytes 1310720 | tf_op jit(solution)/shard_map/all_gather | solution.py:79
  12.3 133.6 %reduce-scatter.3.cloned.1.call-start = ((), (), s32[]{:S(2)}) async-start(), calls=%async_computation.6 | async-start | bytes 1638400 | tf_op jit(solution)/shard_map/reduce_scatter | solution.py:80
  58.8 29.6 %copy-start.6 = (bf16[320,2048]{1,0:T(8,128)(2,1)S(1)}, bf16[320,2048]{1,0:T(8,128)(2,1)}, u32[]{:S(2)}) copy-start(bf16[320,2048]{1,0:T(8,128)(2,1)} %all-gather.8.cloned.1.call-done) | copy-start | bytes 3932164
  97.8 22.3 %copy-start.3 = (bf16[2048]{0:T(1024)(128)(2,1)S(1)}, bf16[2048]{0:T(1024)(128)(2,1)}, u32[]{:S(2)}) copy-start(bf16[2048]{0:T(1024)(128)(2,1)} %param.21) | copy-start | bytes 12292
  97.8 22.3 %copy-start.4 = (bf16[2048]{0:T(1024)(128)(2,1)S(1)}, bf16[2048]{0:T(1024)(128)(2,1)}, u32[]{:S(2)}) copy-start(bf16[2048]{0:T(1024)(128)(2,1)} %param.22) | copy-start | bytes 12292
  97.8 49.3 %copy-start.1 = (bf16[80,2048]{1,0:T(8,128)(2,1)S(1)}, bf16[80,2048]{1,0:T(8,128)(2,1)}, u32[]{:S(2)}) copy-start(bf16[80,2048]{1,0:T(8,128)(2,1)} %param.14) | copy-start | bytes 983044
  120.0 219.4 %all-gather.16.cloned.1.call-start = ((), (), s32[]{:S(2)}) async-start(), calls=%async_computation.7 | async-start | bytes 1638400 | tf_op jit(solution)/shard_map/all_gather | solution.py:90
  149.3 1.6 copy-start
  149.3 125.9 %copy-start.2 = (bf16[2,3,5120]{2,0,1:T(2,128)(2,1)S(1)}, bf16[2,3,5120]{2,0,1:T(2,128)(2,1)}, u32[]{:S(2)}) copy-start(bf16[2,3,5120]{2,0,1:T(2,128)(2,1)} %param.25) | copy-start | bytes 184324
  149.4 190.1 %all-gather.18.cloned.1.call-start = ((), (), s32[]{:S(2)}) async-start(), calls=%async_computation.8 | async-start | bytes 6553600 | tf_op jit(solution)/shard_map/all_gather | solution.py:94
  150.1 266.1 %all-gather.20.cloned.1.call-start = ((), (), s32[]{:S(2)}) async-start(), calls=%async_computation.9 | async-start | bytes 6553600 | tf_op jit(solution)/shard_map/all_gather | solution.py:95
  150.9 302.2 %reduce-scatter.5.cloned.1.call-start = ((), (), s32[]{:S(2)}) async-start(), calls=%async_computation.10 | async-start | bytes 1638400 | tf_op jit(solution)/shard_map/reduce_scatter | solution.py:110
  150.9 33.7 %collective-permute-start = (bf16[1280,512]{1,0:T(8,128)(2,1)S(1)}, bf16[1280,512]{1,0:T(8,128)(2,1)S(1)}, u32[]{:S(2)}, u32[]{:S(2)}) collective-permute-start(bf16[1280,512]{1,0:T(8,128)(2,1)S(1)} %copy-done), channel_id=1, source_target_pairs={{0,4},{4,8},{8,12},{12,0},{1,5},{5,9},{9,13},{13,1},{2,6},{6,10},{... | collective-permute-start | bytes 3932168 | tf_op jit(solution)/shard_map/ppermute | solution.py:106
  184.6 61.5 %collective-permute-start.1 = (bf16[1280,512]{1,0:T(8,128)(2,1)S(1)}, bf16[1280,512]{1,0:T(8,128)(2,1)}, u32[]{:S(2)}, u32[]{:S(2)}) collective-permute-start(bf16[1280,512]{1,0:T(8,128)(2,1)S(1)} %collective-permute-done), channel_id=1, source_target_pairs={{0,4},{4,8},{8,12},{12,0},{1,5},{5,9},{9,13},{13,1},{2,6},{6,10},{... | collective-permute-start | bytes 3932168 | tf_op jit(solution)/shard_map/ppermute | solution.py:106
  246.1 77.8 %collective-permute-start.2 = (bf16[1280,512]{1,0:T(8,128)(2,1)}, bf16[1280,512]{1,0:T(8,128)(2,1)}, u32[]{:S(2)}, u32[]{:S(2)}) collective-permute-start(bf16[1280,512]{1,0:T(8,128)(2,1)} %collective-permute-done.1), channel_id=1, source_target_pairs={{0,4},{4,8},{8,12},{12,0},{1,5},{5,9},{9,13},{13,1},{2,6},{6,10},{... | collective-permute-start | bytes 3932168 | tf_op jit(solution)/shard_map/ppermute | solution.py:106
  422.6 5.5 %copy-start.5 = (bf16[2048]{0:T(1024)(128)(2,1)S(1)}, bf16[2048]{0:T(1024)(128)(2,1)}, u32[]{:S(2)}) copy-start(bf16[2048]{0:T(1024)(128)(2,1)} %param.27) | copy-start | bytes 12292
Sparse Core Ops, SparseCore 0:
  8.9 30.7 all-gather.9
  41.2 17.5 all-gather.7
  60.4 27.9 all-gather.11
  89.8 27.3 all-gather.13
  120.1 25.7 reduce-scatter.2
  149.5 18.1 all-gather.15
  169.3 147.2 all-gather.17
  318.2 98.0 all-gather.19
  428.2 24.7 reduce-scatter.4
